TPU v7x, 32 devices: a whole 2x2x4 slice. The times are simulated.
32 devices in a mesh: sp: 8 (over z, y), tp: 4 (over x, core).
Axes of the slice: x: 2, y: 2, z: 4, core: 2. Of those that a mesh axis runs over, the one named last changes fastest.
Arguments:
- resid: bfloat16 [4096, 2048], P('sp', 'tp'), may hold values from -41 to 41
- queries: bfloat16 [4096, 1024], P('sp', 'tp'), may hold values from -6 to 6
- keys: bfloat16 [4096, 1024], P('sp', 'tp'), may hold values from -6 to 6
- values: bfloat16 [4096, 1024], P('sp', 'tp'), may hold values from -6 to 6
- mix_lambda: float32 [8], P('tp'), may hold values from 0.3 to 0.8
- head_gain: float32 [128], replicated, may hold values from 0.1 to 1.9
- out_weight: bfloat16 [1024, 2048], P(None, 'tp'), may hold values from -0.1875 to 0.1875
- norm_gain: float32 [2048], P('tp'), may hold values from 0.1 to 1.9
- gate_weight: bfloat16 [2048, 5632], P('sp', 'tp'), may hold values from -0.125 to 0.125
- up_weight: bfloat16 [2048, 5632], P('sp', 'tp'), may hold values from -0.125 to 0.125
- conv_weight: float32 [3, 5632], P(None, 'tp'), may hold values from -3.5 to 3.5
- conv_bias: float32 [5632], P('tp'), may hold values from -3 to 3
- down_weight: bfloat16 [5632, 2048], P('tp', 'sp'), may hold values from -0.078125 to 0.078125
Outputs:
- layer_out: bfloat16 [4096, 2048], P('sp', 'tp')
All inputs are finite; a program needn't handle non-finite values.
Results may differ from a plain program's by a relative error of at most 0.009.
Values may be sent and summed in bfloat16 or wider, within the bound.
A program may use at most 128 MiB of HBM per device.

v0:
```python
import math

import jax
import jax.numpy as jnp
from jax import lax
from jax.sharding import PartitionSpec as P

D = 2048
HD = 64
VD = 128


def with_halo(cells, sides, width):
    for axis, dim in sides:
        count = lax.axis_size(axis)
        ends = count - 1
        head = lax.slice_in_dim(cells, 0, width, axis=dim)
        tail = lax.slice_in_dim(cells, cells.shape[dim] - width, cells.shape[dim], axis=dim)
        cells = jnp.concatenate(
            [
                lax.ppermute(tail, axis, [(i, (i + 1) % count) for i in range(ends)]),
                cells,
                lax.ppermute(head, axis, [((i + 1) % count, i) for i in range(ends)]),
            ],
            axis=dim,
        )
    return cells


def on_device(
    resid,
    queries,
    keys,
    values,
    mix_lambda,
    head_gain,
    out_weight,
    norm_gain,
    gate_weight,
    up_weight,
    conv_weight,
    conv_bias,
    down_weight,
):
    length = queries.shape[0]
    heads = mix_lambda.shape[0]
    scale = HD ** (-0.5)
    query_heads = queries.reshape(length, heads, 2, HD)
    initial = (
        jnp.full((heads, 2, length), -1e30, jnp.float32),
        jnp.zeros((heads, 2, length), jnp.float32),
        jnp.zeros((heads, 2, length, VD), jnp.float32),
    )
    key_rows = lax.all_gather(keys, "sp", axis=0, tiled=True)
    value_rows = lax.all_gather(values, "sp", axis=0, tiled=True)
    count = key_rows.shape[0]
    block = math.gcd(count, 2048)
    key_blocks = key_rows.reshape(count // block, block, heads, 2, HD)
    value_blocks = value_rows.reshape(count // block, block, heads, VD)

    def advance(state, blocks):
        running, totals, weighted = state
        key_block, value_block = blocks
        scores = (
            jnp.einsum(
                "qhmd,khmd->hmqk", query_heads, key_block, preferred_element_type=jnp.float32
            )
            * scale
        )
        highest = jnp.maximum(running, jnp.max(scores, axis=-1))
        factor = jnp.exp(running - highest)
        shifted = jnp.exp(scores - highest[..., None])
        totals = totals * factor + jnp.sum(shifted, axis=-1)
        weighted = weighted * factor[..., None] + jnp.einsum(
            "hmqk,khe->hmqe",
            shifted.astype(jnp.bfloat16),
            value_block,
            preferred_element_type=jnp.float32,
        )
        return ((highest, totals, weighted), None)

    result, unused = lax.scan(advance, initial, (key_blocks, value_blocks))
    running, totals, weighted = result
    mapped = weighted / totals[..., None]
    mixed = mapped[:, 0] - mix_lambda[:, None, None] * mapped[:, 1]
    spread = jnp.mean(mixed * mixed, axis=-1, keepdims=True)
    normed = mixed * lax.rsqrt(spread + 1e-06) * head_gain * 0.8
    heads_out = jnp.transpose(normed, (1, 0, 2)).reshape(length, heads * VD).astype(jnp.bfloat16)
    projected = jnp.dot(
        lax.all_gather(heads_out, "tp", axis=1, tiled=True),
        out_weight,
        preferred_element_type=jnp.float32,
    )
    after_mixer = resid.astype(jnp.float32) + projected
    squares = lax.psum(jnp.sum(after_mixer * after_mixer, axis=1), "tp")
    normed_rows = (after_mixer * lax.rsqrt(squares / D + 1e-06)[:, None] * norm_gain).astype(
        jnp.bfloat16
    )
    full_rows = lax.all_gather(normed_rows, "tp", axis=1, tiled=True)
    gate_sum = jnp.dot(
        full_rows,
        lax.all_gather(gate_weight, "sp", axis=0, tiled=True),
        preferred_element_type=jnp.float32,
    )
    upward = jnp.dot(
        full_rows,
        lax.all_gather(up_weight, "sp", axis=0, tiled=True),
        preferred_element_type=jnp.float32,
    )
    gated = gate_sum.astype(jnp.bfloat16)
    padded = with_halo(gated, (("sp", 0),), 1).astype(jnp.float32)
    conv = (
        padded[:-2] * conv_weight[0]
        + padded[1:-1] * conv_weight[1]
        + padded[2:] * conv_weight[2]
        + conv_bias
    )
    hidden = (jax.nn.silu(conv) * upward).astype(jnp.bfloat16)
    partial_terms = jnp.dot(
        hidden,
        lax.all_gather(down_weight, "sp", axis=1, tiled=True),
        preferred_element_type=jnp.float32,
    )
    mixer_out = lax.psum_scatter(
        partial_terms.astype(jnp.bfloat16), "tp", scatter_dimension=1, tiled=True
    ).astype(jnp.float32)
    return (after_mixer + mixer_out).astype(jnp.bfloat16)


def solution(mesh):
    placed = (
        P("sp", "tp"),
        P("sp", "tp"),
        P("sp", "tp"),
        P("sp", "tp"),
        P("tp"),
        P(),
        P(None, "tp"),
        P("tp"),
        P("sp", "tp"),
        P("sp", "tp"),
        P(None, "tp"),
        P("tp"),
        P("tp", "sp"),
    )
    return jax.shard_map(
        on_device, mesh=mesh, in_specs=placed, out_specs=P("sp", "tp"), check_vma=False
    )
```

profile of v0, /device:TPU:0, one launch (start us, length us, event | category | flops | bytes accessed | tf_op | source)
XLA Modules:
  0.0 553.9 jit_solution(7031731348143616948)
XLA Ops:
  6.5 0.0 copy-start
  6.5 0.7 all-gather.8.cloned.1.call-update
  7.3 0.0 all-gather.10.cloned.1.call-start
  7.3 0.7 all-gather.10.cloned.1.call-update
  8.0 0.0 all-gather.12.cloned.1.call-start
  8.1 1.1 copy.23
  9.2 52.1 %all-gather.8.cloned.1.call-done = bf16[4096,256]{1,0:T(8,128)(2,1)} async-done(((bf16[512,256]{1,0:T(8,128)(2,1)}), bf16[4096,256]{1,0:T(8,128)(2,1)}) %all-gather.8.cloned.1.call-update) | async-done | bytes 2097168 | tf_op jit(solution)/shard_map/all_gather | solution.py:54
  61.3 8.3 %reshape.31 = bf16[2,2048,2,2,64]{4,3,2,1,0:T(2,128)(2,1)} reshape(bf16[4096,256]{1,0:T(8,128)(2,1)} %all-gather.8.cloned.1.call-done) | data formatting | bytes 4194304 | tf_op jit(solution)/shard_map/reshape | solution.py:58
  69.6 10.7 %copy.24 = bf16[2,2048,2,2,64]{1,4,3,2,0:T(8,128)(2,1)} copy(bf16[2,2048,2,2,64]{4,3,2,1,0:T(2,128)(2,1)} %reshape.31) | data formatting | bytes 4194304
  80.3 30.7 %all-gather.10.cloned.1.call-done = bf16[4096,256]{1,0:T(8,128)(2,1)} async-done(((bf16[512,256]{1,0:T(8,128)(2,1)}), bf16[4096,256]{1,0:T(8,128)(2,1)}) %all-gather.10.cloned.1.call-update) | async-done | bytes 2097168 | tf_op jit(solution)/shard_map/all_gather | solution.py:55
  111.1 4.0 reshape.29
  115.0 53.5 %while.15 = (s32[]{:T(128)}, f32[2,2,512]{2,1,0:T(2,128)S(1)}, f32[2,2,512]{2,1,0:T(2,128)S(1)}, f32[2,2,512,128]{3,2,1,0:T(8,128)S(1)}, bf16[2,2048,2,2,64]{1,4...) while((s32[]{:T(128)}, f32[2,2,512]{2,1,0:T(2,128)S(1)}, ...), condition=%wide.region_3.4_spmd.clone, body=%wide.region_0.3_spmd.clone.sunk | while | flops 1644963840 | bytes 65405572 | solution.py:82
  115.0 9.3 %bitcast_reduce_fusion.2 = (f32[2,2,512]{2,1,0:T(2,128)S(1)}, f32[2,2,2048,512]{3,2,1,0:T(8,128)}) fusion(bf16[512,2,2,64]{0,3,2,1:T(8,128)(2,1)S(1)} %get-tuple-element.175, bf16[2,2048,2,2,64]{1,4,3,2,0:T(8,128)(2,1)} %get-tuple-element.174, s32[]{:T(128)} %get-tuple-element.161), kind=kOutput, calls=%fused_computation.1.clone.1 | convolution fusion | flops 545257472 | bytes 18096640 | tf_op jit(solution)/shard_map/while/body/eval_jaxpr/qhmd,khmd->hmqk/dot_general | solution.py:65
  124.4 0.0 copy-start.1
  124.4 8.6 %fusion.40 = f32[2,2,512]{2,1,0:T(2,128)S(1)} fusion(f32[2,2,2048,512]{3,2,1,0:T(8,128)} %get-tuple-element.149, f32[2,2,512]{2,1,0:T(2,128)S(1)} %fusion.39), kind=kLoop, calls=%fused_computation.4.clone.1 | loop fusion | flops 12580864 | bytes 16793600 | tf_op jit(solution)/shard_map/while/body/eval_jaxpr/reduce_sum | solution.py:73
  133.1 0.0 copy-done.1
  133.1 0.8 constant_dynamic-slice_fusion.2
  133.9 7.9 %fusion.42 = f32[2,2,512,128]{3,2,1,0:T(8,128)S(1)} fusion(f32[2,2,2048,512]{3,2,1,0:T(8,128)} %get-tuple-element.149, f32[2,2,512]{2,1,0:T(2,128)S(1)} %fusion.39, bf16[1,2048,2,128]{3,2,1,0:T(2,128)(2,1)S(1)} %constant_dynamic-slice_fusion.2, f32[2,2,512,128]{3,2,1,0:T(8,128)S(1)} %get-tuple-element.164, f32[2,2,512]{2,1,0:T(2,128)S(1)} %get-tuple-element.151, ...), kind=kOutput, calls=%fused_computation.6.clone.1 | convolution fusion | flops 1087111168 | bytes 19939328 | tf_op jit(solution)/shard_map/while/body/eval_jaxpr/hmqk,khe->hmqe/dot_general | solution.py:74
  141.8 9.3 %bitcast_reduce_fusion.2 = (f32[2,2,512]{2,1,0:T(2,128)S(1)}, f32[2,2,2048,512]{3,2,1,0:T(8,128)}) fusion(bf16[512,2,2,64]{0,3,2,1:T(8,128)(2,1)S(1)} %get-tuple-element.175, bf16[2,2048,2,2,64]{1,4,3,2,0:T(8,128)(2,1)} %get-tuple-element.174, s32[]{:T(128)} %get-tuple-element.161), kind=kOutput, calls=%fused_computation.1.clone.1 | convolution fusion | flops 545257472 | bytes 18096640 | tf_op jit(solution)/shard_map/while/body/eval_jaxpr/qhmd,khmd->hmqk/dot_general | solution.py:65
  151.2 8.6 %fusion.40 = f32[2,2,512]{2,1,0:T(2,128)S(1)} fusion(f32[2,2,2048,512]{3,2,1,0:T(8,128)} %get-tuple-element.149, f32[2,2,512]{2,1,0:T(2,128)S(1)} %fusion.39), kind=kLoop, calls=%fused_computation.4.clone.1 | loop fusion | flops 12580864 | bytes 16793600 | tf_op jit(solution)/shard_map/while/body/eval_jaxpr/reduce_sum | solution.py:73
  159.8 0.8 constant_dynamic-slice_fusion.2
  160.6 7.9 %fusion.42 = f32[2,2,512,128]{3,2,1,0:T(8,128)S(1)} fusion(f32[2,2,2048,512]{3,2,1,0:T(8,128)} %get-tuple-element.149, f32[2,2,512]{2,1,0:T(2,128)S(1)} %fusion.39, bf16[1,2048,2,128]{3,2,1,0:T(2,128)(2,1)S(1)} %constant_dynamic-slice_fusion.2, f32[2,2,512,128]{3,2,1,0:T(8,128)S(1)} %get-tuple-element.164, f32[2,2,512]{2,1,0:T(2,128)S(1)} %get-tuple-element.151, ...), kind=kOutput, calls=%fused_computation.6.clone.1 | convolution fusion | flops 1087111168 | bytes 19939328 | tf_op jit(solution)/shard_map/while/body/eval_jaxpr/hmqk,khe->hmqe/dot_general | solution.py:74
  168.5 0.0 copy-start.5
  168.6 0.0 copy-start.6
  168.6 0.3 copy.27
  168.9 0.0 copy-start.2
  168.9 0.2 broadcast_divide_fusion
  169.1 0.1 copy-done.5
  169.2 0.2 multiply_reduce_fusion.1
  169.4 0.9 multiply_convert_fusion.1
  170.3 0.0 all-gather.12.cloned.1.call-update
  170.3 0.2 all-gather.14.cloned.1.call-start
  170.5 0.2 copy.21
  170.8 0.0 copy-start.4
  170.8 14.9 %all-gather.12.cloned.1.call-done = bf16[512,1024]{0,1:T(8,128)(2,1)} async-done(((bf16[512,256]{0,1:T(8,128)(2,1)}), bf16[512,1024]{0,1:T(8,128)(2,1)}) %all-gather.12.cloned.1.call-update) | async-done | bytes 1048592 | tf_op jit(solution)/shard_map/all_gather | solution.py:90
  185.7 2.0 multiply_reduce_fusion
  187.7 5.9 %psum.7 = f32[512]{0:T(512)S(1)} all-reduce(f32[512]{0:T(512)S(1)} %get-tuple-element.99), channel_id=1, replica_groups=mesh['sp'=8,'tp'=4] {'tp'}, use_global_device_ids=true, to_apply=%region_6.7 | all-reduce | flops 512 | bytes 4096 | tf_op jit(solution)/shard_map/psum | solution.py:95
  193.6 0.9 multiply_convert_fusion
  194.5 0.0 all-gather.14.cloned.1.call-update
  194.6 0.0 all-gather.16.cloned.1.call-start
  194.6 0.5 all-gather.16.cloned.1.call-update
  195.1 0.0 all-gather.18.cloned.1.call-start
  195.2 0.5 all-gather.18.cloned.1.call-update
  195.7 0.0 all-gather.20.cloned.1.call-start
  195.8 0.7 all-gather.20.cloned.1.call-update
  196.5 0.0 copy-start.3
  196.5 0.0 reduce-scatter.2.cloned.1.call-start
  196.5 21.8 %all-gather.14.cloned.1.call-done = bf16[512,2048]{0,1:T(8,128)(2,1)} async-done(((bf16[512,512]{0,1:T(8,128)(2,1)}), bf16[512,2048]{0,1:T(8,128)(2,1)}) %all-gather.14.cloned.1.call-update) | async-done | bytes 2097168 | tf_op jit(solution)/shard_map/all_gather | solution.py:99
  218.3 94.4 %all-gather.16.cloned.1.call-done = bf16[2048,1408]{1,0:T(8,128)(2,1)} async-done(((bf16[256,1408]{1,0:T(8,128)(2,1)}), bf16[2048,1408]{1,0:T(8,128)(2,1)}) %all-gather.16.cloned.1.call-update) | async-done | bytes 5767184 | tf_op jit(solution)/shard_map/all_gather | solution.py:102
  312.7 6.7 %convolution_convert_fusion = bf16[512,1408]{1,0:T(8,128)(2,1)S(1)} fusion(bf16[512,2048]{0,1:T(8,128)(2,1)} %all-gather.14.cloned.1.call-done, bf16[2048,1408]{1,0:T(8,128)(2,1)} %all-gather.16.cloned.1.call-done), kind=kOutput, calls=%fused_computation.22 | convolution fusion | flops 2953510912 | bytes 9306112 | tf_op jit(solution)/shard_map/dot_general | solution.py:100
  319.4 0.0 copy-start.7
  319.5 2.5 collective-permute-start
  321.9 1.3 collective-permute-start.1
  323.3 0.1 slice_reduce_fusion.2
  323.3 0.0 collective-permute-done
  323.3 4.4 collective-permute-done.1
  327.7 2.0 maximum_convert_fusion
  329.7 75.6 %all-gather.18.cloned.1.call-done = bf16[2048,1408]{1,0:T(8,128)(2,1)} async-done(((bf16[256,1408]{1,0:T(8,128)(2,1)}), bf16[2048,1408]{1,0:T(8,128)(2,1)}) %all-gather.18.cloned.1.call-update) | async-done | bytes 5767184 | tf_op jit(solution)/shard_map/all_gather | solution.py:107
  405.3 93.4 %all-gather.20.cloned.1.call-done = bf16[1408,2048]{1,0:T(8,128)(2,1)} async-done(((bf16[1408,256]{1,0:T(8,128)(2,1)}), bf16[1408,2048]{1,0:T(8,128)(2,1)}) %all-gather.20.cloned.1.call-update) | async-done | bytes 5767184 | tf_op jit(solution)/shard_map/all_gather | solution.py:121
  498.7 16.7 %convolution_convert_fusion.1 = bf16[512,2048]{0,1:T(8,128)(2,1)} fusion(bf16[1408,2048]{1,0:T(8,128)(2,1)} %all-gather.20.cloned.1.call-done, bf16[512,2048]{0,1:T(8,128)(2,1)} %all-gather.14.cloned.1.call-done, bf16[2048,1408]{1,0:T(8,128)(2,1)} %all-gather.18.cloned.1.call-done, f32[514,1408]{1,0:T(8,128)} %maximum_convert_fusion, ...), kind=kOutput, calls=%fused_computation.23 | convolution fusion | flops 5915279360 | bytes 24401920 | tf_op jit(solution)/shard_map/dot_general | solution.py:119
  515.4 0.0 reduce-scatter.2.cloned.1.call-update
  515.4 29.5 %reduce-scatter.2.cloned.1.call-done = bf16[512,512]{0,1:T(8,128)(2,1)} async-done(((bf16[512,2048]{0,1:T(8,128)(2,1)}), bf16[512,512]{0,1:T(8,128)(2,1)}) %reduce-scatter.2.cloned.1.call-update) | async-done | bytes 524304 | tf_op jit(solution)/shard_map/reduce_scatter | solution.py:124
  544.9 1.2 add_convert_fusion
  546.1 1.0 copy.29
  (22 shorter events, 0.1 us)
Async XLA Ops:
  6.5 179.2 %copy-start = (bf16[1024,512]{1,0:T(8,128)(2,1)S(1)}, bf16[1024,512]{1,0:T(8,128)(2,1)}, u32[]{:S(2)}) copy-start(bf16[1024,512]{1,0:T(8,128)(2,1)} %param.21) | copy-start | bytes 3145732
  6.5 54.8 %all-gather.8.cloned.1.call-start = ((), (), s32[]{:S(2)}) async-start(), calls=%async_computation.1 | async-start | bytes 2359296 | tf_op jit(solution)/shard_map/all_gather | solution.py:54
  7.3 103.8 %all-gather.10.cloned.1.call-start = ((), (), s32[]{:S(2)}) async-start(), calls=%async_computation.2 | async-start | bytes 2359296 | tf_op jit(solution)/shard_map/all_gather | solution.py:55
  8.0 177.7 %all-gather.12.cloned.1.call-start = ((), (), s32[]{:S(2)}) async-start(), calls=%async_computation.3 | async-start | bytes 1310720 | tf_op jit(solution)/shard_map/all_gather | solution.py:90
  124.4 8.7 %copy-start.1 = (bf16[2,2048,2,128]{3,2,1,0:T(2,128)(2,1)S(1)}, bf16[2,2048,2,128]{3,2,1,0:T(2,128)(2,1)}, u32[]{:S(2)}) copy-start(bf16[2,2048,2,128]{3,2,1,0:T(2,128)(2,1)} %get-tuple-element.176) | copy-start | bytes 6291460 | tf_op jit(solution)/shard_map/while
  151.1 8.7 %copy-start.1 = (bf16[2,2048,2,128]{3,2,1,0:T(2,128)(2,1)S(1)}, bf16[2,2048,2,128]{3,2,1,0:T(2,128)(2,1)}, u32[]{:S(2)}) copy-start(bf16[2,2048,2,128]{3,2,1,0:T(2,128)(2,1)} %get-tuple-element.176) | copy-start | bytes 6291460 | tf_op jit(solution)/shard_map/while
  168.5 0.7 copy-start.5
  168.6 0.8 copy-start.6
  168.9 1.6 copy-start.2
  170.3 48.0 %all-gather.14.cloned.1.call-start = ((), (), s32[]{:S(2)}) async-start(), calls=%async_computation.4 | async-start | bytes 2621440 | tf_op jit(solution)/shard_map/all_gather | solution.py:99
  170.8 22.8 %copy-start.4 = (f32[512]{0:T(512)S(1)}, f32[512]{0:T(512)}, u32[]{:S(2)}) copy-start(f32[512]{0:T(512)} %param.22) | copy-start | bytes 6148
  194.6 118.2 %all-gather.16.cloned.1.call-start = ((), (), s32[]{:S(2)}) async-start(), calls=%async_computation.5 | async-start | bytes 6488064 | tf_op jit(solution)/shard_map/all_gather | solution.py:102
  195.1 210.1 %all-gather.18.cloned.1.call-start = ((), (), s32[]{:S(2)}) async-start(), calls=%async_computation.6 | async-start | bytes 6488064 | tf_op jit(solution)/shard_map/all_gather | solution.py:107
  195.7 302.9 %all-gather.20.cloned.1.call-start = ((), (), s32[]{:S(2)}) async-start(), calls=%async_computation.7 | async-start | bytes 6488064 | tf_op jit(solution)/shard_map/all_gather | solution.py:121
  196.5 126.8 %copy-start.3 = (f32[3,1408]{1,0:T(4,128)S(1)}, f32[3,1408]{1,0:T(4,128)}, u32[]{:S(2)}) copy-start(f32[3,1408]{1,0:T(4,128)} %param.25) | copy-start | bytes 50692
  196.5 348.4 %reduce-scatter.2.cloned.1.call-start = ((), (), s32[]{:S(2)}) async-start(), calls=%async_computation.8 | async-start | bytes 2621440 | tf_op jit(solution)/shard_map/reduce_scatter | solution.py:124
  319.4 179.2 %copy-start.7 = (f32[1408]{0:T(1024)S(1)}, f32[1408]{0:T(1024)}, u32[]{:S(2)}) copy-start(f32[1408]{0:T(1024)} %param.26) | copy-start | bytes 16900
  319.5 3.8 collective-permute-start
  321.9 5.8 %collective-permute-start.1 = (bf16[1,1408]{1,0:T(2,128)(2,1)S(1)}, bf16[1,1408]{1,0:T(2,128)(2,1)S(1)}, u32[]{:S(2)}, u32[]{:S(2)}) collective-permute-start(bf16[1,1408]{1,0:T(2,128)(2,1)S(1)} %get-tuple-element.98), channel_id=1, source_target_pairs={{4,0},{8,4},{12,8},{16,12},{20,16},{24,20},{28,24},{5,1},{9,5},{13... | collective-permute-start | bytes 8456 | tf_op jit(solution)/shard_map/ppermute | solution.py:23
Sparse Core Ops, SparseCore 0:
  9.5 51.7 all-gather.7
  63.4 47.6 all-gather.9
  170.4 15.2 all-gather.11
  194.7 23.6 all-gather.13
  220.4 92.3 all-gather.15
  314.7 90.4 all-gather.17
  407.3 91.2 all-gather.19
  515.5 29.3 reduce-scatter.1
where the time goes:
time: 555 us; the launch traced here: 554 us
  waiting for transfers between devices  420 us (76%)
  matrix products  59.9 us (11%)
  local copies, waits for them, and re-layouts  27.4 us (5%)
  other arithmetic  22.7 us (4%)
  between operations  13.7 us (2%)
  blocking collectives  5.88 us (1%)
    all_gather x1, waiting for transfers between devices, on_device(): lax.all_gather(gate_weight, 'sp', axis=0, tiled=True)  94.4 us
    all_gather x1, waiting for transfers between devices, on_device(): lax.all_gather(down_weight, 'sp', axis=1, tiled=True)  93.4 us
    all_gather x1, waiting for transfers between devices, on_device(): lax.all_gather(up_weight, 'sp', axis=0, tiled=True)  75.6 us
    all_gather x1, waiting for transfers between devices, on_device(): key_rows = lax.all_gather(keys, 'sp', axis=0, tiled=True)  52.1 us
    all_gather x1, waiting for transfers between devices, on_device(): value_rows = lax.all_gather(values, 'sp', axis=0, tiled=True)  30.7 us
    reduce_scatter x1, waiting for transfers between devices, on_device(): lax.psum_scatter(partial_terms.astype(jnp.bfloat16), 'tp', scatter_dimens...  29.5 us
    all_gather x1, waiting for transfers between devices, on_device(): full_rows = lax.all_gather(normed_rows, 'tp', axis=1, tiled=True)  21.8 us
    dot_general x2, matrix products, advance(): jnp.einsum('qhmd,khmd->hmqk', query_heads, key_block, preferred_element_t...  18.7 us
  transfers between devices with their start and end apart: 10, of which 9 were waited for; matrix products, arithmetic and copies ran while one was open for 5% of the time, Pallas kernels for 0%

commit v1 on v0

--- a/solution.py
+++ b/solution.py
@@ -1,8 +1,11 @@
+import functools
 import math
 
 import jax
 import jax.numpy as jnp
 from jax import lax
+from jax.experimental import pallas as pl
+from jax.experimental.pallas import tpu as pltpu
 from jax.sharding import PartitionSpec as P
 
 D = 2048
@@ -127,7 +130,482 @@
     return (after_mixer + mixer_out).astype(jnp.bfloat16)
 
 
+PAIR, LINE = 0, 1
+EDGE = 16
+
+
+def layer_kernel(
+    sp,
+    tp,
+    resid,
+    queries,
+    keys,
+    values,
+    mix_lambda,
+    head_gain,
+    out_weight,
+    norm_gain,
+    gate_weight,
+    up_weight,
+    conv_weight,
+    conv_bias,
+    down_weight,
+    out,
+    kv,
+    gates,
+    ups,
+    downs,
+    peaks,
+    totals,
+    weighted,
+    heads_all,
+    after,
+    square_all,
+    rows_all,
+    gate_acc,
+    up_acc,
+    hidden,
+    partials,
+    landed,
+    local_sem,
+    kv_send,
+    kv_recv,
+    w_send,
+    w_recv,
+    head_send,
+    head_recv,
+    square_send,
+    square_recv,
+    row_send,
+    row_recv,
+    edge_send,
+    edge_recv,
+    part_send,
+    part_recv,
+):
+    bf16, f32 = jnp.bfloat16, jnp.float32
+    me = lax.axis_index("sp")
+    t = lax.axis_index("tp")
+    nz = sp // 2
+    z, y = me // 2, lax.rem(me, 2)
+    length = queries.shape[0]
+    heads = queries.shape[1] // VD
+    half_k = gate_weight.shape[0] // 2
+    half_f = down_weight.shape[0] // 2
+    weights = (gates, ups, downs)
+
+    local = [
+        pltpu.make_async_copy(keys, kv.at[me, 0], local_sem.at[0]),
+        pltpu.make_async_copy(values, kv.at[me, 1], local_sem.at[1]),
+    ]
+    for i, ref in enumerate((gate_weight, up_weight)):
+        for h in range(2):
+            local.append(
+                pltpu.make_async_copy(
+                    ref.at[pl.ds(h * half_k, half_k)],
+                    weights[i].at[me, h],
+                    local_sem.at[2 + 2 * i + h],
+                )
+            )
+    for h in range(2):
+        local.append(
+            pltpu.make_async_copy(
+                down_weight.at[pl.ds(h * half_f, half_f)], downs.at[me, h], local_sem.at[6 + h]
+            )
+        )
+    for copy in local:
+        copy.start()
+
+    def routes(kind, zs, ys):
+        if kind == PAIR:
+            up = jnp.logical_and(zs <= z, z < nz - 1)
+            down = jnp.logical_and(zs >= z, z > 0)
+            across = jnp.logical_and(zs == z, ys == y)
+        else:
+            up = jnp.logical_and(ys == y, jnp.logical_and(zs <= z, z < nz - 1))
+            down = jnp.logical_and(ys == y, jnp.logical_and(zs >= z, z > 0))
+            across = ys == y
+        return (
+            (up, jnp.minimum(me + 2, sp - 1)),
+            (down, jnp.maximum(me - 2, 0)),
+            (across, 2 * z + 1 - y),
+        )
+
+    def remote(ref, send, recv, target):
+        return pltpu.make_async_remote_copy(
+            src_ref=ref,
+            dst_ref=ref,
+            send_sem=send,
+            recv_sem=recv,
+            device_id={"sp": target},
+            device_id_type=pl.DeviceIdType.MESH,
+        )
+
+    def kv_copy(kind, src, way, target):
+        return remote(kv.at[src, kind], kv_send.at[kind, way, src], kv_recv.at[kind, src], target)
+
+    def w_copy(array, kind, src, way, target):
+        return remote(
+            weights[array].at[src, kind],
+            w_send.at[array, kind, way, src],
+            w_recv.at[array, kind, src],
+            target,
+        )
+
+    def push(make, kind, src, ways=(0, 1, 2), wait=False):
+        zs, ys = src // 2, lax.rem(src, 2)
+        plan = routes(kind, zs, ys)
+        for way in ways:
+            needed, target = plan[way]
+
+            @pl.when(needed)
+            def _():
+                copy = make(kind, src, way, target)
+                if wait:
+                    copy.wait_send()
+                else:
+                    copy.start()
+
+    def take(make, kind, src):
+        @pl.when(src != me)
+        def _():
+            make(kind, src, 0, lax.rem(me + 2, sp)).wait_recv()
+            push(make, kind, src)
+
+    def visit(body, after_ring=None):
+        def event(e, carry):
+            d = e // 4
+            above = lax.rem(e // 2, 2)
+            ys = lax.rem(y + lax.rem(e, 2), 2)
+            zs = jnp.where(above == 1, z + d, z - d)
+            valid = jnp.logical_and(jnp.logical_and(zs >= 0, zs < nz), d + (1 - above) > 0)
+
+            @pl.when(valid)
+            def _():
+                body(2 * zs + ys)
+
+            if after_ring is not None:
+
+                @pl.when(lax.rem(e, 4) == 3)
+                def _():
+                    after_ring(d)
+
+            return carry
+
+        lax.fori_loop(0, 4 * nz, event, 0)
+
+    for copy in local:
+        copy.wait()
+    push(kv_copy, PAIR, me)
+    push(kv_copy, LINE, me)
+
+    peaks[...] = jnp.full(peaks.shape, -1e30, f32)
+    totals[...] = jnp.zeros(totals.shape, f32)
+    weighted[...] = jnp.zeros(weighted.shape, f32)
+    lanes = lax.broadcasted_iota(jnp.int32, (1, 2 * HD), 1)
+    scale = HD**-0.5
+    rows = math.gcd(length, 256)
+
+    def attend(src):
+        take(kv_copy, PAIR, src)
+        take(kv_copy, LINE, src)
+
+        def row_block(r, carry):
+            at = pl.ds(pl.multiple_of(r * rows, rows), rows)
+            for h in range(heads):
+                cols = slice(h * VD, (h + 1) * VD)
+                q = queries[at, cols].astype(f32) * scale
+                key_block = kv[src, 0, :, cols]
+                value_block = kv[src, 1, :, cols]
+                for m in range(2):
+                    keep = lanes < HD if m == 0 else lanes >= HD
+                    qm = jnp.where(keep, q, 0.0).astype(bf16)
+                    s = lax.dot_general(
+                        qm, key_block, (((1,), (1,)), ((), ())), preferred_element_type=f32
+                    )
+                    i = 2 * h + m
+                    old = peaks[i, at, :]
+                    new = jnp.maximum(old, jnp.max(s, axis=1, keepdims=True))
+                    factor = jnp.exp(old - new)
+                    p = jnp.exp(s - new)
+                    peaks[i, at, :] = new
+                    totals[i, at, :] = totals[i, at, :] * factor + jnp.sum(
+                        p, axis=1, keepdims=True
+                    )
+                    weighted[i, at, :] = weighted[i, at, :] * factor + jnp.dot(
+                        p.astype(bf16), value_block, preferred_element_type=f32
+                    )
+            return carry
+
+        lax.fori_loop(0, length // rows, row_block, 0)
+
+    def feed(d):
+        for way, turn in ((0, z), (1, nz - 1 - z), (2, nz - 1)):
+
+            @pl.when(d == turn)
+            def _():
+                for array in range(3):
+                    for kind in (PAIR, LINE):
+                        push(functools.partial(w_copy, array), kind, me, (way,))
+
+    visit(attend, feed)
+
+    for h in range(heads):
+        first = weighted[2 * h] / totals[2 * h]
+        second = weighted[2 * h + 1] / totals[2 * h + 1]
+        mixed = first - mix_lambda[h] * second
+        spread = jnp.mean(mixed * mixed, axis=1, keepdims=True)
+        normed = mixed * lax.rsqrt(spread + 1e-06) * head_gain[...] * 0.8
+        heads_all[t, :, h * VD : (h + 1) * VD] = normed.astype(bf16)
+
+    def to_peers(ref_of, send, recv):
+        copies = []
+        for j in range(1, tp):
+            copy = pltpu.make_async_remote_copy(
+                src_ref=ref_of,
+                dst_ref=ref_of,
+                send_sem=send.at[j],
+                recv_sem=recv.at[j],
+                device_id={"tp": lax.rem(t + j, tp)},
+                device_id_type=pl.DeviceIdType.MESH,
+            )
+            copy.start()
+            copies.append(copy)
+        return copies
+
+    sent = to_peers(heads_all.at[t], head_send, head_recv)
+    for copy in sent:
+        copy.wait()
+    width = heads * VD
+    total = resid[...].astype(f32)
+    for j in range(tp):
+        total = total + jnp.dot(
+            heads_all[j], out_weight[j * width : (j + 1) * width, :], preferred_element_type=f32
+        )
+    after[...] = total
+    row_sum = jnp.sum(total * total, axis=1, keepdims=True)
+    square_all[t] = jnp.transpose(jnp.broadcast_to(row_sum, (length, 128)))[:8]
+    sent = to_peers(square_all.at[t], square_send, square_recv)
+    for copy in sent:
+        copy.wait()
+    summed = square_all[0]
+    for j in range(1, tp):
+        summed = summed + square_all[j]
+    inverse = lax.rsqrt(summed / D + 1e-06)
+    inverse = jnp.transpose(jnp.concatenate([inverse] * 16, axis=0))[:, :1]
+    rows_all[t, EDGE : EDGE + length, :] = (after[...] * inverse * norm_gain[...]).astype(bf16)
+    sent = to_peers(rows_all.at[t, pl.ds(EDGE, length)], row_send, row_recv)
+    for copy in sent:
+        copy.wait()
+
+    def edge_copy(way, source, dest, target):
+        return pltpu.make_async_remote_copy(
+            src_ref=rows_all.at[:, pl.ds(source, EDGE)],
+            dst_ref=rows_all.at[:, pl.ds(dest, EDGE)],
+            send_sem=edge_send.at[way],
+            recv_sem=edge_recv.at[way],
+            device_id={"sp": target},
+            device_id_type=pl.DeviceIdType.MESH,
+        )
+
+    onward = edge_copy(0, length, 0, jnp.minimum(me + 1, sp - 1))
+    back = edge_copy(1, EDGE, EDGE + length, jnp.maximum(me - 1, 0))
+    not_last, not_first = me < sp - 1, me > 0
+
+    @pl.when(not_last)
+    def _():
+        onward.start()
+
+    @pl.when(not_first)
+    def _():
+        back.start()
+
+    @pl.when(me == 0)
+    def _():
+        rows_all[:, 0:EDGE, :] = jnp.zeros((tp, EDGE, rows_all.shape[2]), bf16)
+
+    @pl.when(me == sp - 1)
+    def _():
+        rows_all[:, EDGE + length :, :] = jnp.zeros((tp, EDGE, rows_all.shape[2]), bf16)
+
+    @pl.when(not_first)
+    def _():
+        onward.wait_recv()
+
+    @pl.when(not_last)
+    def _():
+        back.wait_recv()
+
+    gate_acc[...] = jnp.zeros(gate_acc.shape, f32)
+    up_acc[...] = jnp.zeros(up_acc.shape, f32)
+    per = sp // tp
+    depth = 2 * half_k
+    ff = gate_weight.shape[1]
+
+    def expand(src):
+        for array in range(2):
+            for kind in (PAIR, LINE):
+                take(functools.partial(w_copy, array), kind, src)
+        cols = pl.ds(pl.multiple_of(lax.rem(src, per) * depth, depth), depth)
+        x = rows_all[src // per, :, cols]
+        gate_acc[...] += jnp.dot(
+            x, gates[src].reshape(depth, ff), preferred_element_type=f32
+        )
+        up_acc[...] += jnp.dot(
+            x[EDGE : EDGE + length], ups[src].reshape(depth, ff), preferred_element_type=f32
+        )
+
+    visit(expand)
+
+    for c in range(0, ff, 128):
+        cols = slice(c, c + 128)
+
+        def tap(start):
+            return gate_acc[start : start + length, cols].astype(bf16).astype(f32)
+
+        conv = (
+            tap(EDGE - 1) * conv_weight[0:1, cols]
+            + tap(EDGE) * conv_weight[1:2, cols]
+            + tap(EDGE + 1) * conv_weight[2:3, cols]
+            + conv_bias[:, cols]
+        )
+        hidden[:, cols] = (conv / (1.0 + jnp.exp(-conv)) * up_acc[:, cols]).astype(bf16)
+
+    def part_copy(src, owner, sender):
+        return pltpu.make_async_remote_copy(
+            src_ref=partials.at[src],
+            dst_ref=landed.at[sender, lax.rem(src, per)],
+            send_sem=part_send.at[src],
+            recv_sem=part_recv.at[sender, lax.rem(src, per)],
+            device_id={"tp": owner},
+            device_id_type=pl.DeviceIdType.MESH,
+        )
+
+    def contract(src):
+        for kind in (PAIR, LINE):
+            take(functools.partial(w_copy, 2), kind, src)
+        part = jnp.dot(
+            hidden[...],
+            downs[src].reshape(2 * half_f, downs.shape[3]),
+            preferred_element_type=f32,
+        )
+        partials[src] = part.astype(bf16)
+        owner = src // per
+
+        @pl.when(owner != t)
+        def _():
+            part_copy(src, owner, t).start()
+
+    visit(contract)
+
+    wide = partials.shape[2]
+    for q in range(per):
+        cols = slice(q * wide, (q + 1) * wide)
+        total = partials[t * per + q].astype(f32)
+        for j in range(1, tp):
+            sender = lax.rem(t + j, tp)
+            part_copy(t * per + q, sender, sender).wait_recv()
+            total = total + landed[sender, q].astype(f32)
+        out[:, cols] = (after[:, cols] + total).astype(bf16)
+
+    @pl.when(not_last)
+    def _():
+        onward.wait_send()
+
+    @pl.when(not_first)
+    def _():
+        back.wait_send()
+
+    def drain(src, carry):
+        for kind in (PAIR, LINE):
+            push(kv_copy, kind, src, wait=True)
+            for array in range(3):
+                push(functools.partial(w_copy, array), kind, src, wait=True)
+
+        @pl.when(src // per != t)
+        def _():
+            part_copy(src, src // per, t).wait_send()
+
+        return carry
+
+    lax.fori_loop(0, sp, drain, 0)
+
+
+def fused(sp, tp, *args):
+    resid, queries, keys, values = args[:4]
+    gate_weight, down_weight = args[8], args[12]
+    length, width = queries.shape
+    features = resid.shape[1]
+    depth, ff = gate_weight.shape
+    maps = 2 * (width // VD)
+    bf16, f32 = jnp.bfloat16, jnp.float32
+    dma = pltpu.SemaphoreType.DMA
+    vmem = pl.BlockSpec(memory_space=pltpu.VMEM)
+    smem = pl.BlockSpec(memory_space=pltpu.SMEM)
+    hbm = pl.BlockSpec(memory_space=pl.ANY)
+    rows = length + 2 * EDGE
+    down_cols = down_weight.shape[1]
+    args = list(args)
+    for i in (5, 7, 11):
+        args[i] = args[i].reshape(1, -1)
+    return pl.pallas_call(
+        functools.partial(layer_kernel, sp, tp),
+        out_shape=jax.ShapeDtypeStruct(resid.shape, bf16),
+        in_specs=[
+            vmem, vmem, hbm, hbm, smem, vmem, vmem, vmem, hbm, hbm, vmem, vmem, hbm,
+        ],
+        out_specs=vmem,
+        scratch_shapes=[
+            pltpu.VMEM((sp, 2, length, width), bf16),
+            pltpu.VMEM((sp, 2, depth // 2, ff), bf16),
+            pltpu.VMEM((sp, 2, depth // 2, ff), bf16),
+            pltpu.VMEM((sp, 2, ff // 2, down_cols), bf16),
+            pltpu.VMEM((maps, length, 1), f32),
+            pltpu.VMEM((maps, length, 1), f32),
+            pltpu.VMEM((maps, length, VD), f32),
+            pltpu.VMEM((tp, length, width), bf16),
+            pltpu.VMEM((length, features), f32),
+            pltpu.VMEM((tp, 8, length), f32),
+            pltpu.VMEM((tp, rows, features), bf16),
+            pltpu.VMEM((rows, ff), f32),
+            pltpu.VMEM((length, ff), f32),
+            pltpu.VMEM((length, ff), bf16),
+            pltpu.VMEM((sp, length, down_cols), bf16),
+            pltpu.VMEM((tp, sp // tp, length, down_cols), bf16),
+            dma((8,)),
+            dma((2, 3, sp)),
+            dma((2, sp)),
+            dma((3, 2, 3, sp)),
+            dma((3, 2, sp)),
+            dma((tp,)),
+            dma((tp,)),
+            dma((tp,)),
+            dma((tp,)),
+            dma((tp,)),
+            dma((tp,)),
+            dma((2,)),
+            dma((2,)),
+            dma((sp,)),
+            dma((tp, sp // tp)),
+        ],
+        compiler_params=pltpu.CompilerParams(
+            has_side_effects=True, vmem_limit_bytes=60 * 1024 * 1024
+        ),
+    )(*args)
+
+
 def solution(mesh):
+    sp, tp = mesh.shape["sp"], mesh.shape["tp"]
+
+    def run(*args):
+        width, depth = args[1].shape[1], args[8].shape[0]
+        small = args[0].shape[0] <= 512
+        whole_pairs = sp % 2 == 0 and sp % tp == 0
+        if whole_pairs and small and depth % 256 == 0 and width % VD == 0:
+            return fused(sp, tp, *args)
+        return on_device(*args)
+
+
     placed = (
         P("sp", "tp"),
         P("sp", "tp"),
@@ -144,5 +622,5 @@
         P("tp", "sp"),
     )
     return jax.shard_map(
-        on_device, mesh=mesh, in_specs=placed, out_specs=P("sp", "tp"), check_vma=False
-    )
+        run, mesh=mesh, in_specs=placed, out_specs=P("sp", "tp"), check_vma=False
+    )

time: 555 us -> 309 us (0.56)
  waiting for transfers between devices: 420 us -> 0 us
  Pallas kernels: 0 us -> 305 us
  matrix products: 59.9 us -> 0 us
  local copies, waits for them, and re-layouts: 27.4 us -> 3.16 us
  other arithmetic: 22.7 us -> 0 us
  between operations: 13.7 us -> 0.01 us
  blocking collectives: 5.88 us -> 0 us
    all_gather x7 -> x0, waiting for transfers between devices: 383 us -> none  [the longest x1 94.4 us: on_device(): lax.all_gather(gate_weight, 'sp', axis=0, tiled=True)]
    pallas_call x0 -> x1, Pallas kernels: none -> 305 us  [fused(): pl.pallas_call(functools.partial(layer_kernel, sp, tp), out_shape=jax.Sha...]
    dot_general x7 -> x0, matrix products: 59.9 us -> none  [the longest x2 18.7 us: advance(): jnp.einsum('qhmd,khmd->hmqk', query_heads, key_block, preferred_element_t...]
    reduce_scatter x1 -> x0, waiting for transfers between devices: 29.5 us -> none  [on_device(): lax.psum_scatter(partial_terms.astype(jnp.bfloat16), 'tp', scatter_dimens...]
    reduce_sum x3 -> x0, other arithmetic: 17.5 us -> none  [the longest x2 17.3 us: advance(): totals = totals * factor + jnp.sum(shifted, axis=-1)]
    reshape x2 -> x1, local copies, waits for them, and re-layouts: 12.3 us -> 1.29 us  [fused(): args[i] = args[i].reshape(1, -1)]
    unnamed x17 -> x1, local copies, waits for them, and re-layouts: 12.2 us -> 1.87 us
    psum x1 -> x0, blocking collectives: 5.88 us -> none  [on_device(): squares = lax.psum(jnp.sum(after_mixer * after_mixer, axis=1), 'tp')]
  transfers between devices with their start and end apart: 10 -> 0, of which waited for: 9 -> 0; matrix products, arithmetic and copies ran while one was open for 5% -> 0% of each run, Pallas kernels for 0% -> 0%
where the time goes in v1:
time: 309 us; the launch traced here: 308 us
  Pallas kernels  305 us (99%)
  local copies, waits for them, and re-layouts  3.16 us (1%)
    pallas_call x1, Pallas kernels, fused(): pl.pallas_call(functools.partial(layer_kernel, sp, tp), out_shape=jax.Sha...  305 us

profile of v1, /device:TPU:0, one launch (start us, length us, event | category | flops | bytes accessed | tf_op | source)
XLA Modules:
  0.0 308.4 jit_solution(2066966436663786997)
XLA Ops:
  0.0 1.3 reshape.11.conv_bias
  1.3 305.2 %shard_map.127 = bf16[512,512]{1,0:T(8,128)(2,1)} custom-call(bf16[512,512]{1,0:T(8,128)(2,1)} %resid.1, bf16[512,256]{1,0:T(8,128)(2,1)} %queries.1, bf16[512,256]{1,0:T(8,128)(2,1)} %keys.1, bf16[512,256]{1,0:T(8,128)(2,1)} %values.1, f32[2]{0:T(128)} %mix_lambda.1, f32[1,128]{1,0:T(1,128)} %bitcast.3, bf16[1024,512]{1,0:T(8,128)(2,1)} %out_weight.1, ...), custom_call_target="tpu_custom_call" | custom-call | tf_op jit(solution)/shard_map/pallas_call | solution.py:551
  306.6 1.9 copy.15

commit v2 on v1

--- a/solution.py
+++ b/solution.py
@@ -272,11 +272,11 @@
             make(kind, src, 0, lax.rem(me + 2, sp)).wait_recv()
             push(make, kind, src)
 
-    def visit(body, after_ring=None):
+    def visit(first, last, body, after_ring=None):
         def event(e, carry):
             d = e // 4
-            above = lax.rem(e // 2, 2)
-            ys = lax.rem(y + lax.rem(e, 2), 2)
+            above = lax.rem(e, 2)
+            ys = lax.rem(y + lax.rem(e // 2, 2), 2)
             zs = jnp.where(above == 1, z + d, z - d)
             valid = jnp.logical_and(jnp.logical_and(zs >= 0, zs < nz), d + (1 - above) > 0)
 
@@ -292,7 +292,7 @@
 
             return carry
 
-        lax.fori_loop(0, 4 * nz, event, 0)
+        lax.fori_loop(4 * first, 4 * last, event, 0)
 
     for copy in local:
         copy.wait()
@@ -348,7 +348,7 @@
                     for kind in (PAIR, LINE):
                         push(functools.partial(w_copy, array), kind, me, (way,))
 
-    visit(attend, feed)
+    visit(0, nz, attend, feed)
 
     for h in range(heads):
         first = weighted[2 * h] / totals[2 * h]
@@ -358,24 +358,46 @@
         normed = mixed * lax.rsqrt(spread + 1e-06) * head_gain[...] * 0.8
         heads_all[t, :, h * VD : (h + 1) * VD] = normed.astype(bf16)
 
-    def to_peers(ref_of, send, recv):
+    core = lax.rem(t, 2)
+    sibling = t + 1 - 2 * core
+    half_tp = tp // 2
+
+    def tp_copy(ref, send, recv, target):
+        return pltpu.make_async_remote_copy(
+            src_ref=ref,
+            dst_ref=ref,
+            send_sem=send,
+            recv_sem=recv,
+            device_id={"tp": target},
+            device_id_type=pl.DeviceIdType.MESH,
+        )
+
+    def spread(slot, send, recv):
         copies = []
-        for j in range(1, tp):
-            copy = pltpu.make_async_remote_copy(
-                src_ref=ref_of,
-                dst_ref=ref_of,
-                send_sem=send.at[j],
-                recv_sem=recv.at[j],
-                device_id={"tp": lax.rem(t + j, tp)},
-                device_id_type=pl.DeviceIdType.MESH,
+        for k in range(1, half_tp):
+            copies.append(tp_copy(slot(t), send.at[k], recv.at[k], lax.rem(t + 2 * k, tp)))
+            copies[-1].start()
+        copies.append(tp_copy(slot(t), send.at[0], recv.at[0], sibling))
+        copies[-1].start()
+        return copies
+
+    def settle(slot, send, recv, copies):
+        for k in range(1, half_tp):
+            copies[k - 1].wait_recv()
+            came = lax.rem(t + tp - 2 * k, tp)
+            copies.append(
+                tp_copy(slot(came), send.at[half_tp + k], recv.at[half_tp + k], sibling)
             )
-            copy.start()
-            copies.append(copy)
-        return copies
-
-    sent = to_peers(heads_all.at[t], head_send, head_recv)
-    for copy in sent:
-        copy.wait()
+            copies[-1].start()
+        for copy in copies[half_tp - 1 :]:
+            copy.wait_recv()
+        for copy in copies:
+            copy.wait_send()
+
+    def exchange(slot, send, recv):
+        settle(slot, send, recv, spread(slot, send, recv))
+
+    exchange(lambda j: heads_all.at[j], head_send, head_recv)
     width = heads * VD
     total = resid[...].astype(f32)
     for j in range(tp):
@@ -385,18 +407,23 @@
     after[...] = total
     row_sum = jnp.sum(total * total, axis=1, keepdims=True)
     square_all[t] = jnp.transpose(jnp.broadcast_to(row_sum, (length, 128)))[:8]
-    sent = to_peers(square_all.at[t], square_send, square_recv)
-    for copy in sent:
-        copy.wait()
+    exchange(lambda j: square_all.at[j], square_send, square_recv)
     summed = square_all[0]
     for j in range(1, tp):
         summed = summed + square_all[j]
     inverse = lax.rsqrt(summed / D + 1e-06)
     inverse = jnp.transpose(jnp.concatenate([inverse] * 16, axis=0))[:, :1]
     rows_all[t, EDGE : EDGE + length, :] = (after[...] * inverse * norm_gain[...]).astype(bf16)
-    sent = to_peers(rows_all.at[t, pl.ds(EDGE, length)], row_send, row_recv)
-    for copy in sent:
-        copy.wait()
+    own_rows = lambda j: rows_all.at[j, pl.ds(EDGE, length)]
+    sent = spread(own_rows, row_send, row_recv)
+
+    def relay(src):
+        for array in range(3):
+            for kind in (PAIR, LINE):
+                take(functools.partial(w_copy, array), kind, src)
+
+    visit(0, 1, relay)
+    settle(own_rows, row_send, row_recv, sent)
 
     def edge_copy(way, source, dest, target):
         return pltpu.make_async_remote_copy(
@@ -428,6 +455,8 @@
     def _():
         rows_all[:, EDGE + length :, :] = jnp.zeros((tp, EDGE, rows_all.shape[2]), bf16)
 
+    visit(1, 2, relay)
+
     @pl.when(not_first)
     def _():
         onward.wait_recv()
@@ -443,9 +472,6 @@
     ff = gate_weight.shape[1]
 
     def expand(src):
-        for array in range(2):
-            for kind in (PAIR, LINE):
-                take(functools.partial(w_copy, array), kind, src)
         cols = pl.ds(pl.multiple_of(lax.rem(src, per) * depth, depth), depth)
         x = rows_all[src // per, :, cols]
         gate_acc[...] += jnp.dot(
@@ -455,7 +481,12 @@
             x[EDGE : EDGE + length], ups[src].reshape(depth, ff), preferred_element_type=f32
         )
 
-    visit(expand)
+    def relay_expand(src):
+        relay(src)
+        expand(src)
+
+    visit(0, 2, expand)
+    visit(2, nz, relay_expand)
 
     for c in range(0, ff, 128):
         cols = slice(c, c + 128)
@@ -471,42 +502,56 @@
         )
         hidden[:, cols] = (conv / (1.0 + jnp.exp(-conv)) * up_acc[:, cols]).astype(bf16)
 
-    def part_copy(src, owner, sender):
+    def part(owner, q):
+        return jnp.dot(
+            hidden[...],
+            downs[owner * per + q].reshape(2 * half_f, downs.shape[3]),
+            preferred_element_type=f32,
+        )
+
+    def part_copy(slot, q, target):
         return pltpu.make_async_remote_copy(
-            src_ref=partials.at[src],
-            dst_ref=landed.at[sender, lax.rem(src, per)],
-            send_sem=part_send.at[src],
-            recv_sem=part_recv.at[sender, lax.rem(src, per)],
-            device_id={"tp": owner},
+            src_ref=partials.at[slot, q],
+            dst_ref=landed.at[slot, q],
+            send_sem=part_send.at[slot, q],
+            recv_sem=part_recv.at[slot, q],
+            device_id={"tp": target},
             device_id_type=pl.DeviceIdType.MESH,
         )
 
-    def contract(src):
-        for kind in (PAIR, LINE):
-            take(functools.partial(w_copy, 2), kind, src)
-        part = jnp.dot(
-            hidden[...],
-            downs[src].reshape(2 * half_f, downs.shape[3]),
-            preferred_element_type=f32,
-        )
-        partials[src] = part.astype(bf16)
-        owner = src // per
-
-        @pl.when(owner != t)
-        def _():
-            part_copy(src, owner, t).start()
-
-    visit(contract)
-
-    wide = partials.shape[2]
+    shipped = []
+    for k in range(1, half_tp):
+        chip = lax.rem(t // 2 + k, half_tp)
+        for q in range(per):
+            partials[half_tp + k, q] = part(2 * chip + 1 - core, q).astype(bf16)
+            copy = part_copy(half_tp + k, q, sibling)
+            copy.start()
+            shipped.append(copy)
+        for q in range(per):
+            mine = part(2 * chip + core, q)
+            shipped[(k - 1) * 2 * per + q].wait_recv()
+            partials[k, q] = (mine + landed[half_tp + k, q].astype(f32)).astype(bf16)
+            copy = part_copy(k, q, 2 * chip + core)
+            copy.start()
+            shipped.append(copy)
+    for q in range(per):
+        partials[0, q] = part(sibling, q).astype(bf16)
+        copy = part_copy(0, q, sibling)
+        copy.start()
+        shipped.append(copy)
+    wide = partials.shape[3]
     for q in range(per):
         cols = slice(q * wide, (q + 1) * wide)
-        total = partials[t * per + q].astype(f32)
-        for j in range(1, tp):
-            sender = lax.rem(t + j, tp)
-            part_copy(t * per + q, sender, sender).wait_recv()
-            total = total + landed[sender, q].astype(f32)
-        out[:, cols] = (after[:, cols] + total).astype(bf16)
+        after[:, cols] += part(t, q)
+    for q in range(per):
+        cols = slice(q * wide, (q + 1) * wide)
+        total = after[:, cols]
+        for k in range(half_tp):
+            part_copy(k, q, sibling).wait_recv()
+            total = total + landed[k, q].astype(f32)
+        out[:, cols] = total.astype(bf16)
+    for copy in shipped:
+        copy.wait_send()
 
     @pl.when(not_last)
     def _():
@@ -521,10 +566,6 @@
             push(kv_copy, kind, src, wait=True)
             for array in range(3):
                 push(functools.partial(w_copy, array), kind, src, wait=True)
-
-        @pl.when(src // per != t)
-        def _():
-            part_copy(src, src // per, t).wait_send()
 
         return carry
 
@@ -570,7 +611,7 @@
             pltpu.VMEM((rows, ff), f32),
             pltpu.VMEM((length, ff), f32),
             pltpu.VMEM((length, ff), bf16),
-            pltpu.VMEM((sp, length, down_cols), bf16),
+            pltpu.VMEM((tp, sp // tp, length, down_cols), bf16),
             pltpu.VMEM((tp, sp // tp, length, down_cols), bf16),
             dma((8,)),
             dma((2, 3, sp)),
@@ -585,7 +626,7 @@
             dma((tp,)),
             dma((2,)),
             dma((2,)),
-            dma((sp,)),
+            dma((tp, sp // tp)),
             dma((tp, sp // tp)),
         ],
         compiler_params=pltpu.CompilerParams(
@@ -600,7 +641,7 @@
     def run(*args):
         width, depth = args[1].shape[1], args[8].shape[0]
         small = args[0].shape[0] <= 512
-        whole_pairs = sp % 2 == 0 and sp % tp == 0
+        whole_pairs = sp % 2 == 0 and tp % 2 == 0 and sp % tp == 0
         if whole_pairs and small and depth % 256 == 0 and width % VD == 0:
             return fused(sp, tp, *args)
         return on_device(*args)

time: 309 us -> 305 us (0.987)
    pallas_call x1, Pallas kernels: 305 us -> 302 us  [fused(): pl.pallas_call(functools.partial(layer_kernel, sp, tp), out_shape=jax.Sha...]
where the time goes in v2:
time: 305 us
  Pallas kernels  302 us (99%)
  local copies, waits for them, and re-layouts  3.16 us (1%)
    pallas_call x1, Pallas kernels, fused(): pl.pallas_call(functools.partial(layer_kernel, sp, tp), out_shape=jax.Sha...  302 us

profile of v2, /device:TPU:0, one launch (start us, length us, event | category | flops | bytes accessed | tf_op | source)
XLA Modules:
  0.0 304.7 jit_solution(16250074076778548218)
XLA Ops:
  0.0 1.3 reshape.11.conv_bias
  1.3 301.5 %shard_map.127 = bf16[512,512]{1,0:T(8,128)(2,1)} custom-call(bf16[512,512]{1,0:T(8,128)(2,1)} %resid.1, bf16[512,256]{1,0:T(8,128)(2,1)} %queries.1, bf16[512,256]{1,0:T(8,128)(2,1)} %keys.1, bf16[512,256]{1,0:T(8,128)(2,1)} %values.1, f32[2]{0:T(128)} %mix_lambda.1, f32[1,128]{1,0:T(1,128)} %bitcast.3, bf16[1024,512]{1,0:T(8,128)(2,1)} %out_weight.1, ...), custom_call_target="tpu_custom_call" | custom-call | tf_op jit(solution)/shard_map/pallas_call | solution.py:592
  302.8 1.9 copy.15
